TPU v7x, 512 devices: a 8x2x16 block of a 8x8x16 slice. The times are simulated.
512 devices in a mesh: grp: 2 (over y), sp: 16 (over z), dp: 16 (over x, core).
Axes of the slice: x: 8, y: 2, z: 16, core: 2. Of those that a mesh axis runs over, the one named last changes fastest.
The devices are a block of a 8x8x16 slice.
Arguments:
- tokens: bfloat16 [32, 2560, 2048], P(('grp', 'dp'), 'sp'), parts along dimension 0, may hold values from -6 to 6
- query_weight: bfloat16 [2048, 1024], P('dp'), may hold values from -0.125 to 0.125
- key_weight: bfloat16 [2048, 256], P('dp'), may hold values from -0.125 to 0.125
- value_weight: bfloat16 [2048, 256], P('dp'), may hold values from -0.125 to 0.125
- out_weight: bfloat16 [1024, 2048], P(None, 'dp'), may hold values from -0.1875 to 0.1875
- query_gain: float32 [64], replicated, may hold values from 0.28 to 6
- key_gain: float32 [64], replicated, may hold values from 0.28 to 6
Outputs:
- mixed: bfloat16 [32, 2560, 2048], P(('grp', 'dp'), 'sp'), parts along dimension 0
There are 2 independent parts, one for each index of `grp`. A program takes and returns all parts, laid end to end along the dimension named above; an argument that names none is the same for every part. Nothing has to cross between parts.
All inputs are finite; a program needn't handle non-finite values.
Results may differ from a plain program's by a relative error of at most 0.006.
The roundings to bfloat16 on the way count: a program that leaves them out, or rounds other values in their place, can miss the bound.
Values may be sent and summed in bfloat16 or wider, within the bound.
A program may use at most 64 MiB of HBM per device.

v0:
```python
import jax
import jax.numpy as jnp
from jax import lax
from jax.sharding import PartitionSpec as P

HEADS = 16
KV_HEADS = 4
HEAD_DIM = 64
GRID_W = 64


theta_base = 10000.0
norm_eps = 1e-06


def sent_together(arrays, axis, dim, along):
    ends, at = ([], 0)
    for a in arrays[:-1]:
        at += a.shape[along]
        ends.append(at)
    both = jnp.concatenate(arrays, axis=along)
    return tuple(jnp.split(lax.all_gather(both, axis, axis=dim, tiled=True), ends, axis=along))


def rotary_tables(positions):
    quarter = HEAD_DIM // 4
    inverse = theta_base ** (-jnp.arange(quarter, dtype=jnp.float32) / quarter)
    grid_rows = (positions // GRID_W).astype(jnp.float32)
    grid_cols = (positions % GRID_W).astype(jnp.float32)
    angles = jnp.concatenate([grid_rows[:, None] * inverse, grid_cols[:, None] * inverse], axis=-1)
    return (jnp.cos(angles), jnp.sin(angles))


def norm_rotate(raw, gain, cosine, sine):
    scaled = raw * lax.rsqrt(jnp.mean(raw * raw, axis=-1, keepdims=True) + norm_eps) * gain
    half = HEAD_DIM // 2
    first_half = scaled[..., :half]
    second_half = scaled[..., half:]
    cosine = cosine[:, None, :]
    sine = sine[:, None, :]
    turned = jnp.concatenate(
        [first_half * cosine - second_half * sine, second_half * cosine + first_half * sine],
        axis=-1,
    )
    return turned.astype(jnp.bfloat16)


def attend_block(queries, keys, values):
    scale = HEAD_DIM ** (-0.5)
    scores = jnp.einsum("qkgd,skd->kgqs", queries, keys, preferred_element_type=jnp.float32) * scale
    top = jnp.max(scores, axis=-1, keepdims=True)
    weights = jnp.exp(scores - top)
    probs = (weights / jnp.sum(weights, axis=-1, keepdims=True)).astype(jnp.bfloat16)
    result = jnp.einsum("kgqs,skd->qkgd", probs, values, preferred_element_type=jnp.float32).astype(
        jnp.bfloat16
    )
    return result.reshape(queries.shape[0], -1)


def shards(tokens, query_weight, key_weight, value_weight, out_weight, query_gain, key_gain):
    tok_rows = tokens.shape[1]
    local_rows = tokens.reshape(tok_rows, tokens.shape[2])
    seq_index = lax.axis_index("sp")
    per_kv = HEADS // KV_HEADS
    pieces = sent_together((query_weight, key_weight, value_weight), "dp", 0, 1)
    raw_q, raw_k, raw_v = tuple(
        (jnp.dot(local_rows, piece, preferred_element_type=jnp.float32) for piece in pieces)
    )
    positions = seq_index * tok_rows + jnp.arange(tok_rows, dtype=jnp.int32)
    cosine, sine = rotary_tables(positions)
    queries = norm_rotate(raw_q.reshape(tok_rows, HEADS, HEAD_DIM), query_gain, cosine, sine)
    keys = norm_rotate(raw_k.reshape(tok_rows, KV_HEADS, HEAD_DIM), key_gain, cosine, sine)
    values = raw_v.astype(jnp.bfloat16).reshape(tok_rows, KV_HEADS, HEAD_DIM)
    kv_pair = jnp.stack(
        [
            keys.reshape(tok_rows, KV_HEADS * HEAD_DIM),
            values.reshape(tok_rows, KV_HEADS * HEAD_DIM),
        ],
        axis=1,
    )
    whole_kv = lax.all_gather(kv_pair, "sp", axis=0, tiled=True)
    length = whole_kv.shape[0]
    all_k = whole_kv[:, 0].reshape(length, KV_HEADS, HEAD_DIM).transpose(1, 0, 2)[:, :, None, :]
    all_v = whole_kv[:, 1].reshape(length, KV_HEADS, HEAD_DIM).transpose(1, 0, 2)[:, :, None, :]
    grouped_q = queries.reshape(tok_rows, KV_HEADS, 1, per_kv, HEAD_DIM).transpose(1, 0, 2, 3, 4)

    def kv_head(operands):
        block_q, block_k, block_v = operands
        return attend_block(block_q, block_k, block_v)

    per_head = lax.map(kv_head, (grouped_q, all_k, all_v))
    attended = per_head.transpose(1, 0, 2).reshape(tok_rows, HEADS * HEAD_DIM)
    result = jnp.dot(
        attended,
        lax.all_gather(out_weight, "dp", axis=1, tiled=True),
        preferred_element_type=jnp.float32,
    )
    return result.astype(jnp.bfloat16).reshape(1, tok_rows, result.shape[1])


def solution(mesh):
    in_specs = (
        P(("grp", "dp"), "sp", None),
        P("dp", None),
        P("dp", None),
        P("dp", None),
        P(None, "dp"),
        P(),
        P(),
    )
    out_specs = P(("grp", "dp"), "sp", None)
    return jax.shard_map(shards, mesh=mesh, in_specs=in_specs, out_specs=out_specs, check_vma=False)
```

profile of v0, /device:TPU:65, one launch (start us, length us, event | category | flops | bytes accessed | tf_op | source)
XLA Modules:
  0.0 242.1 jit_solution(6979037957639061434)
XLA Ops:
  6.6 1.8 pad_maximum_fusion
  8.8 88.1 %all-gather.4.cloned.1.call-done = bf16[2048,1536]{1,0:T(8,128)(2,1)} async-done(((bf16[128,1536]{1,0:T(8,128)(2,1)}), bf16[2048,1536]{1,0:T(8,128)(2,1)}) %all-gather.4.cloned.1.call-update) | async-done | bytes 6291472 | tf_op jit(solution)/shard_map/all_gather | solution.py:22
  96.9 1.6 convolution_bitcast_fusion
  98.9 1.6 fusion.23
  102.2 3.0 %fusion.20 = f32[160,1024]{1,0:T(8,128)S(1)} fusion(bf16[2048,1536]{1,0:T(8,128)(2,1)} %all-gather.4.cloned.1.call-done, bf16[1,160,2048]{2,1,0:T(8,128)(2,1)S(1)} %copy-done), kind=kOutput, calls=%fused_computation.27 | convolution fusion | flops 671088640 | bytes 5505024 | tf_op jit(solution)/shard_map/dot_general | solution.py:67
  108.2 0.9 maximum_bitcast_fusion
  109.1 57.9 %all-gather.6.cloned.1.call-done = bf16[2560,2,256]{2,0,1:T(8,128)(2,1)} async-done(((bf16[160,2,256]{2,0,1:T(8,128)(2,1)}), bf16[2560,2,256]{2,0,1:T(8,128)(2,1)}) %all-gather.6.cloned.1.call-update) | async-done | bytes 2621456 | tf_op jit(solution)/shard_map/all_gather | solution.py:81
  167.0 1.9 fusion.34
  168.9 1.6 copy.14
  171.3 27.9 %while.10 = (s32[]{:T(128)}, bf16[4,160,256]{1,2,0:T(8,128)(2,1)}, bf16[4,2560,1,64]{1,3,2,0:T(8,128)(2,1)}, bf16[4,2560,1,64]{1,3,2,0:T(8,128)(2,1)S(1)}, bf16[4,160,1,4,64]{1,4,3,2,0:T(8,128)(2,1)}, /*index=5*/s32[]{:T(128)}) while((s32[]{:T(128)}, bf16[4,160,256]{1,2,0:T(8,128)(2,1)}, bf16[4,2560,1,64]{1,3,2,0:T(8,128)(2,1)}, ...), condition=%wide.region_5.6_spmd, body=%wide.region_2.5_spmd.sunk | while | flops 434215680 | bytes 20757060 | solution.py:91
  171.3 2.1 bitcast_reduce_fusion.2
  173.4 1.2 fusion.43
  174.7 2.9 %fusion.44 = bf16[64,4,160]{2,0,1:T(8,128)(2,1)S(1)} fusion(f32[4,160]{1,0:T(4,128)S(1)} %fusion.43, f32[4,160]{1,0:T(4,128)S(1)} %get-tuple-element.96, f32[2560,160,4]{0,1,2:T(8,128)S(1)} %get-tuple-element.95, bf16[4,2560,1,64]{1,3,2,0:T(8,128)(2,1)} %get-tuple-element.111, s32[]{:T(128)} %get-tuple-element.103), kind=kOutput, calls=%fused_computation.7.clone.1 | convolution fusion | flops 216309760 | bytes 6968832 | tf_op jit(solution)/shard_map/while/body/eval_jaxpr/kgqs,skd->qkgd/dot_general | solution.py:54
  178.2 2.1 bitcast_reduce_fusion.2
  180.4 1.2 fusion.43
  181.6 2.9 %fusion.44 = bf16[64,4,160]{2,0,1:T(8,128)(2,1)S(1)} fusion(f32[4,160]{1,0:T(4,128)S(1)} %fusion.43, f32[4,160]{1,0:T(4,128)S(1)} %get-tuple-element.96, f32[2560,160,4]{0,1,2:T(8,128)S(1)} %get-tuple-element.95, bf16[4,2560,1,64]{1,3,2,0:T(8,128)(2,1)} %get-tuple-element.111, s32[]{:T(128)} %get-tuple-element.103), kind=kOutput, calls=%fused_computation.7.clone.1 | convolution fusion | flops 216309760 | bytes 6968832 | tf_op jit(solution)/shard_map/while/body/eval_jaxpr/kgqs,skd->qkgd/dot_general | solution.py:54
  185.2 2.1 bitcast_reduce_fusion.2
  187.3 1.2 fusion.43
  188.6 2.9 %fusion.44 = bf16[64,4,160]{2,0,1:T(8,128)(2,1)S(1)} fusion(f32[4,160]{1,0:T(4,128)S(1)} %fusion.43, f32[4,160]{1,0:T(4,128)S(1)} %get-tuple-element.96, f32[2560,160,4]{0,1,2:T(8,128)S(1)} %get-tuple-element.95, bf16[4,2560,1,64]{1,3,2,0:T(8,128)(2,1)} %get-tuple-element.111, s32[]{:T(128)} %get-tuple-element.103), kind=kOutput, calls=%fused_computation.7.clone.1 | convolution fusion | flops 216309760 | bytes 6968832 | tf_op jit(solution)/shard_map/while/body/eval_jaxpr/kgqs,skd->qkgd/dot_general | solution.py:54
  192.1 2.2 bitcast_reduce_fusion.2
  194.3 1.2 fusion.43
  195.5 2.9 %fusion.44 = bf16[64,4,160]{2,0,1:T(8,128)(2,1)S(1)} fusion(f32[4,160]{1,0:T(4,128)S(1)} %fusion.43, f32[4,160]{1,0:T(4,128)S(1)} %get-tuple-element.96, f32[2560,160,4]{0,1,2:T(8,128)S(1)} %get-tuple-element.95, bf16[4,2560,1,64]{1,3,2,0:T(8,128)(2,1)} %get-tuple-element.111, s32[]{:T(128)} %get-tuple-element.103), kind=kOutput, calls=%fused_computation.7.clone.1 | convolution fusion | flops 216309760 | bytes 6968832 | tf_op jit(solution)/shard_map/while/body/eval_jaxpr/kgqs,skd->qkgd/dot_general | solution.py:54
  199.1 32.3 %all-gather.8.cloned.1.call-done = bf16[1024,2048]{1,0:T(8,128)(2,1)} async-done(((bf16[1024,128]{1,0:T(8,128)(2,1)}), bf16[1024,2048]{1,0:T(8,128)(2,1)}) %all-gather.8.cloned.1.call-update) | async-done | bytes 4194320 | tf_op jit(solution)/shard_map/all_gather | solution.py:95
  231.5 4.1 %fusion.19 = bf16[1,160,2048]{2,1,0:T(8,128)(2,1)} fusion(bf16[160,1024]{0,1:T(8,128)(2,1)} %bitcast.109, bf16[1024,2048]{1,0:T(8,128)(2,1)} %all-gather.8.cloned.1.call-done), kind=kOutput, calls=%fused_computation.22 | convolution fusion | flops 671416320 | bytes 5177344 | tf_op jit(solution)/shard_map/dot_general | solution.py:93
  (39 shorter events, 8.8 us)
Async XLA Ops:
  6.5 90.3 %copy-start = (bf16[1,160,2048]{2,1,0:T(8,128)(2,1)S(1)}, bf16[1,160,2048]{2,1,0:T(8,128)(2,1)}, u32[]{:S(2)}) copy-start(bf16[1,160,2048]{2,1,0:T(8,128)(2,1)} %param.9) | copy-start | bytes 1966084
  6.6 92.1 %copy-start.1 = (f32[64]{0:T(128)S(1)}, f32[64]{0:T(128)}, u32[]{:S(2)}) copy-start(f32[64]{0:T(128)} %param.15) | copy-start | bytes 772
  6.6 90.3 %all-gather.4.cloned.1.call-start = ((), (), s32[]{:S(2)}) async-start(), calls=%async_computation | async-start | bytes 6684672 | tf_op jit(solution)/shard_map/all_gather | solution.py:22
  8.5 158.6 %all-gather.6.cloned.1.call-start = ((), (), s32[]{:S(2)}) async-start(), calls=%async_computation.1 | async-start | bytes 2785280 | tf_op jit(solution)/shard_map/all_gather | solution.py:81
  101.2 130.2 %all-gather.8.cloned.1.call-start = ((), (), s32[]{:S(2)}) async-start(), calls=%async_computation.2 | async-start | bytes 4456448 | tf_op jit(solution)/shard_map/all_gather | solution.py:95
  105.3 0.8 copy-start.2
Sparse Core Ops, SparseCore 0:
  9.5 87.3 all-gather.3
  101.4 65.6 all-gather.5
  169.1 62.3 all-gather.7
where the time goes:
time: 243 us; the launch traced here: 242 us
  waiting for transfers between devices  179 us (74%)
  matrix products  30.5 us (13%)
  between operations  13.3 us (5%)
  other arithmetic  10.2 us (4%)
  local copies, waits for them, and re-layouts  8.79 us (4%)
    all_gather x1, waiting for transfers between devices, sent_together(): lax.all_gather(both, axis, axis=dim, tiled=True)  88.1 us
    all_gather x1, waiting for transfers between devices, shards(): whole_kv = lax.all_gather(kv_pair, 'sp', axis=0, tiled=True)  57.9 us
    all_gather x1, waiting for transfers between devices, shards(): lax.all_gather(out_weight, 'dp', axis=1, tiled=True)  32.3 us
    dot_general x4, matrix products, attend_block(): jnp.einsum('kgqs,skd->qkgd', probs, values, preferred_element_type=jnp.fl...  11.6 us
    dot_general x4, matrix products, attend_block(): jnp.einsum('qkgd,skd->kgqs', queries, keys, preferred_element_type=jnp.fl...  8.6 us
    dot_general x3, matrix products, shards(): jnp.dot(local_rows, piece, preferred_element_type=jnp.float32)  6.16 us
    reduce_sum x4, other arithmetic, attend_block(): jnp.sum(weights, axis=-1, keepdims=True)  4.88 us
  transfers between devices with their start and end apart: 3, of which 3 were waited for; matrix products, arithmetic and copies ran while one was open for 16% of the time, Pallas kernels for 0%

commit v1 on v0

v1 whole, which is shorter than its diff:
```python
import math

import jax
import jax.numpy as jnp
from jax import lax
from jax.experimental import pallas as pl
from jax.experimental.pallas import tpu as pltpu
from jax.sharding import PartitionSpec as P

HEADS = 16
KV_HEADS = 4
HEAD_DIM = 64
GRID_W = 64
PER_KV = HEADS // KV_HEADS
HALF = HEAD_DIM // 2
QUARTER = HEAD_DIM // 4

theta_base = 10000.0
norm_eps = 1e-06
MESH = pl.DeviceIdType.MESH
ONES = 16
VROWS = HEAD_DIM + ONES

X_KV0, X_KV_STEP = 3.0, 2.9
X_W_STEP = 5.7
Z0, Z_STEP = 15.0, 3.55
UNIT_US = 1.3


def norm_rotate_t(raw, gain, cosine, sine):
    inv = lax.rsqrt(jnp.mean(raw * raw, axis=0, keepdims=True) + norm_eps)
    scaled = raw * inv * gain
    first, second = scaled[:HALF], scaled[HALF:]
    return jnp.concatenate(
        [first * cosine - second * sine, second * cosine + first * sine], axis=0
    )


def make_schedule(nx, nz):
    h, hz = nx // 2, nz // 2
    events = []
    t = X_KV0
    for cls in range(3):
        step = X_KV_STEP if cls == 0 else X_W_STEP
        for s in range(1, h + 1):
            for p in range(2):
                for d in range(2):
                    if s == h and p != d:
                        continue
                    at = t + (s - 1) * step + step * (0.5 + 0.5 * p if s < h else 0.5)
                    events.append((at, "w", cls, d, s, p))
        t += (h - 0.5) * step
    for s in range(1, hz + 1):
        for p in range(2):
            for d in range(2):
                if s == hz and p != d:
                    continue
                at = Z0 + (s - 1) * Z_STEP + Z_STEP * (0.5 + 0.5 * p if s < hz else 0.5) + 0.5
                events.append((at, "z", d, s, p))
    return sorted(events, key=lambda e: e[0])


def kernel(nx, nz, tok_in, wq_in, wk_in, wv_in, wo_in, qg_in, kg_in, out_ref,
           tok, wq, wk, wv, wo, kbuf, vbuf, vt, qbd, rawq, tab, acc, top, att,
           ring_recv, ring_send, d2d_recv, d2d_send, z_recv, z_send, loc):
    h_x, h_z = nx // 2, nz // 2
    rows = tok.shape[0]
    cols = PER_KV * rows
    dp = lax.axis_index("dp")
    z = lax.axis_index("sp")
    x, c = dp // 2, lax.rem(dp, 2)
    other = 1 - c
    to_x = ({"dp": lax.rem(dp + 2, 2 * nx)}, {"dp": lax.rem(dp + 2 * nx - 2, 2 * nx)})
    to_z = ({"sp": lax.rem(z + 1, nz)}, {"sp": lax.rem(z + nz - 1, nz)})
    to_core = {"dp": 2 * x + other}

    wrows = wk.shape[2]
    loads = []

    def load(src, dst):
        cp = pltpu.make_async_copy(src, dst, loc.at[len(loads)])
        cp.start()
        loads.append(cp)

    load(wk_in, wk.at[x, c])
    load(wv_in, wv.at[x, c])
    load(tok_in.at[0], tok)
    for p in range(2):
        load(wq_in.at[pl.ds(p * (wrows // 2), wrows // 2)], wq.at[x, c, p])
    orows = wo.shape[3]
    for p in range(2):
        load(wo_in.at[pl.ds(p * orows, orows)], wo.at[x, c, p])

    barrier = pltpu.get_barrier_semaphore()
    for peer in (*to_x, *to_z, to_core):
        pl.semaphore_signal(barrier, inc=1, device_id=peer, device_id_type=MESH)

    t = lax.broadcasted_iota(jnp.int32, (HALF, cols), 1)
    for _ in range(PER_KV - 1):
        t = jnp.where(t >= rows, t - rows, t)
    pos = z * rows + t
    j = lax.broadcasted_iota(jnp.int32, (HALF, cols), 0)
    on_row = j < QUARTER
    freq = jnp.exp(jnp.where(on_row, j, j - QUARTER).astype(jnp.float32) * (-math.log(theta_base) / QUARTER))
    angle = jnp.where(on_row, pos // GRID_W, lax.rem(pos, GRID_W)).astype(jnp.float32) * freq
    tab[0] = jnp.cos(angle)
    tab[1] = jnp.sin(angle)
    diag = lax.broadcasted_iota(jnp.int32, (HEAD_DIM, HEAD_DIM), 0) == lax.broadcasted_iota(
        jnp.int32, (HEAD_DIM, HEAD_DIM), 1
    )

    def column(ref):
        return jnp.sum(jnp.where(diag, ref[...], 0.0), axis=1, keepdims=True)

    vt[:, HEAD_DIM:, :] = jnp.ones((KV_HEADS, ONES, vt.shape[2]), jnp.bfloat16)
    qbd[...] = jnp.zeros(qbd.shape, jnp.bfloat16)
    acc[...] = jnp.zeros(acc.shape, jnp.float32)
    top[...] = jnp.full(top.shape, -1e30, jnp.float32)

    pl.semaphore_wait(barrier, 5)

    def piece(cls, xi, p):
        if cls == 0:
            return (wk, wv)[p].at[xi, c]
        return (wq, wo)[cls - 1].at[xi, c, p]

    def lane(cls, p):
        return cls + 1 if cls else p

    def ring_copy(cls, d, s, p):
        owner = lax.rem(x + (nx - s + 1 if d == 0 else s - 1), nx)
        ref = piece(cls, owner, p)
        return pltpu.make_async_remote_copy(
            src_ref=ref, dst_ref=ref, send_sem=ring_send.at[cls],
            recv_sem=ring_recv.at[cls, d, s - 1, p],
            device_id=to_x[d], device_id_type=MESH,
        )

    def core_copy(cls, xi, p):
        ref = piece(cls, xi, p)
        pltpu.make_async_remote_copy(
            src_ref=ref, dst_ref=ref, send_sem=d2d_send.at[lane(cls, p)],
            recv_sem=d2d_recv.at[lane(cls, p)],
            device_id=to_core, device_id_type=MESH,
        ).start()

    def start_own(cls):
        for p in range(2):
            for d in range(2):
                ring_copy(cls, d, 1, p).start()
        for p in range(2):
            core_copy(cls, x, p)

    def arrive_w(cls, d, s, p):
        owner = lax.rem(x + (nx - s if d == 0 else s), nx)
        ref = piece(cls, owner, p)
        pltpu.make_async_copy(ref, ref, ring_recv.at[cls, d, s - 1, p]).wait()
        if s + 1 < h_x or (s + 1 == h_x and p == d):
            ring_copy(cls, d, s + 1, p).start()
        core_copy(cls, owner, p)

    def z_slot(d, s):
        return 0 if s == 0 else (2 * s - 1 if d == 0 or s == h_z else 2 * s)

    def z_send_piece(d, s, p):
        buf = (kbuf, vbuf)[p]
        pltpu.make_async_remote_copy(
            src_ref=buf.at[z_slot(d, s - 1)], dst_ref=buf.at[z_slot(d, s)],
            send_sem=z_send.at[p], recv_sem=z_recv.at[d, s - 1, p],
            device_id=to_z[d], device_id_type=MESH,
        ).start()

    def arrive_z(d, s, p):
        ref = (kbuf, vbuf)[p].at[z_slot(d, s)]
        pltpu.make_async_copy(ref, ref, z_recv.at[d, s - 1, p]).wait()
        if s + 1 < h_z or (s + 1 == h_z and p == d):
            z_send_piece(d, s + 1, p)

    def core_wait(i):
        ref = (wk.at[:, other], wv.at[:, other], wq.at[:, other], wo.at[:, other])[i]
        pltpu.make_async_copy(ref, ref, d2d_recv.at[i]).wait()

    def project(weight):
        total = jnp.zeros((rows, weight.shape[-1]), jnp.float32)
        for i in range(nx):
            total += jnp.dot(
                tok[:, 2 * wrows * i:2 * wrows * (i + 1)],
                weight[i].reshape(2 * wrows, weight.shape[-1]),
                preferred_element_type=jnp.float32,
            )
        return total

    def make_kv():
        core_wait(1)
        vbuf[0] = project(wv).astype(jnp.bfloat16)
        core_wait(0)
        raw = project(wk)
        width = KV_HEADS * HEAD_DIM
        padded = jnp.concatenate([raw, jnp.zeros((width - rows, width), jnp.float32)], axis=0).T
        gain = column(kg_in)
        cosine, sine = tab[0, :, :width], tab[1, :, :width]
        turned = jnp.concatenate(
            [
                norm_rotate_t(padded[HEAD_DIM * i:HEAD_DIM * (i + 1)], gain, cosine, sine)
                for i in range(KV_HEADS)
            ],
            axis=0,
        ).T
        kbuf[0] = turned[:rows].astype(jnp.bfloat16)
        for p in (1, 0):
            for d in range(2):
                z_send_piece(d, 1, p)

    def make_q():
        core_wait(2)
        tile = 256

        @pl.loop(0, HEADS * HEAD_DIM // tile)
        def _(n):
            at = pl.ds(pl.multiple_of(n * tile, tile), tile)
            total = jnp.zeros((rows, tile), jnp.float32)
            for i in range(nx):
                total += jnp.dot(
                    tok[:, 2 * wrows * i:2 * wrows * (i + 1)],
                    wq[i, :, :, :, at].reshape(2 * wrows, tile),
                    preferred_element_type=jnp.float32,
                )
            rawq[:, at] = total

        gain = column(qg_in)
        for g in range(KV_HEADS):
            both = jnp.concatenate(
                [rawq[:, 256 * g:256 * g + 128], rawq[:, 256 * g + 128:256 * g + 256]], axis=0
            )
            stacked = jnp.concatenate([both, pltpu.roll(both, 64, 1)], axis=0)
            raw = stacked.T[:HEAD_DIM]
            at = (g % 2) * HEAD_DIM
            qbd[g, at:at + HEAD_DIM, :] = norm_rotate_t(raw, gain, tab[0], tab[1]).astype(jnp.bfloat16)

    factor = HEAD_DIM ** (-0.5) * math.log2(math.e)
    edges = list(range(0, cols, 256)) + [cols]

    def attend(u):
        keys = 2 * rows
        v = vbuf[2 * u:2 * u + 2].reshape(keys, KV_HEADS * HEAD_DIM).astype(jnp.float32)
        v = jnp.concatenate([v, jnp.zeros((vt.shape[2] - keys, v.shape[1]), jnp.float32)], axis=0)
        v = v.T.astype(jnp.bfloat16)
        for g in range(KV_HEADS):
            vt[g, :HEAD_DIM, :] = v[HEAD_DIM * g:HEAD_DIM * (g + 1)]

        @pl.loop(0, KV_HEADS)
        def _(g):
            block = pl.ds(pl.multiple_of((g // 2) * 128, 128), 128)
            k = kbuf[2 * u:2 * u + 2, :, block].reshape(keys, 128)
            for a, b in zip(edges[:-1], edges[1:]):
                s = jnp.dot(k, qbd[g, :, a:b], preferred_element_type=jnp.float32) * factor
                old = top[g, :, a:b]
                new = jnp.maximum(old, jnp.max(s, axis=0, keepdims=True))
                p = jnp.exp2(s - new).astype(jnp.bfloat16)
                o = jnp.dot(vt[g, :, :keys], p, preferred_element_type=jnp.float32)
                acc[g, :, a:b] = acc[g, :, a:b] * jnp.exp2(old - new) + o
                top[g, :, a:b] = new

    def finish():
        for g in range(KV_HEADS):
            o = acc[g, :HEAD_DIM] / acc[g, HEAD_DIM:HEAD_DIM + 1]
            o = jnp.concatenate([o, jnp.zeros((128 - HEAD_DIM, cols), jnp.float32)], axis=0).T
            y = (o[:2 * rows] + pltpu.roll(o[2 * rows:], 64, 1)).astype(jnp.bfloat16)
            att[:, 256 * g:256 * g + 128] = y[:rows]
            att[:, 256 * g + 128:256 * g + 256] = y[rows:]

    def project_out():
        core_wait(3)
        depth = att.shape[1]
        width = 2 * wo.shape[-1]

        @pl.loop(0, nx)
        def _(i):
            w = jnp.concatenate(
                [wo[i, 0].reshape(depth, width // 2), wo[i, 1].reshape(depth, width // 2)], axis=1
            )
            out_ref[0, :, pl.ds(pl.multiple_of(i * width, width), width)] = jnp.dot(
                att[...], w, preferred_element_type=jnp.float32
            ).astype(jnp.bfloat16)

    loads[0].wait()
    loads[1].wait()
    start_own(0)
    for cp in loads[2:]:
        cp.wait()

    left = {0: 0, 1: 0, 2: 0}
    events = make_schedule(nx, nz)
    last_forward = {}
    for e in events:
        if e[1] == "w":
            left[e[2]] += 1
            if e[4] < h_x:
                last_forward[e[2]] = e
    seen_z = {}
    done_units, q_ready, clock = 0, False, 0.0

    def arrived_units():
        n = 0
        while n < h_z:
            need = [(d, s, p) for s in range(1, n + 2) for d in range(2) for p in range(2)
                    if z_slot(d, s) <= 2 * n + 1 and not (s == h_z and p != d)]
            if all(k in seen_z for k in need):
                n += 1
            else:
                break
        return n

    for e in events:
        clock = max(clock, e[0])
        if q_ready and done_units < arrived_units():
            while done_units < arrived_units() and clock + UNIT_US * 0.5 <= e[0] + 0.01 + UNIT_US:
                attend(done_units)
                done_units += 1
                clock += UNIT_US
                break
        if e[1] == "w":
            _, _, cls, d, s, p = e
            arrive_w(cls, d, s, p)
            left[cls] -= 1
            if cls < 2 and e is last_forward[cls]:
                start_own(cls + 1)
            if left[cls] == 0 and cls == 0:
                make_kv()
            if left[cls] == 0 and cls == 1:
                make_q()
                q_ready = True
        else:
            _, _, d, s, p = e
            arrive_z(d, s, p)
            seen_z[(d, s, p)] = True
    while done_units < h_z:
        attend(done_units)
        done_units += 1
    finish()
    project_out()

    def drain(ref, sem):
        pltpu.make_async_copy(ref, ref, sem).wait()

    drain(wk.at[0:nx - 1], ring_send.at[0])
    drain(wq.at[0:nx - 1, 0], ring_send.at[1])
    drain(wo.at[0:nx - 1, 0], ring_send.at[2])
    for i, ref in enumerate((wk, wv, wq, wo)):
        drain(ref.at[:, c], d2d_send.at[i])
    drain(kbuf.at[0:nz - 1], z_send.at[0])
    drain(vbuf.at[0:nz - 1], z_send.at[1])


def shards(nx, nz, tokens, query_weight, key_weight, value_weight, out_weight, query_gain, key_gain):
    rows, width = tokens.shape[1], tokens.shape[2]
    wrows, qcols = query_weight.shape
    kcols = key_weight.shape[1]
    odepth, ocols = out_weight.shape
    cols = PER_KV * rows
    keys = -(-2 * rows // 128) * 128
    bf, f32 = jnp.bfloat16, jnp.float32
    dma = pltpu.SemaphoreType.DMA
    anywhere = pl.BlockSpec(memory_space=pl.ANY)
    vmem = pl.BlockSpec(memory_space=pltpu.VMEM)
    return pl.pallas_call(
        lambda *refs: kernel(nx, nz, *refs),
        out_shape=jax.ShapeDtypeStruct(tokens.shape[:2] + (2 * nx * ocols,), bf),
        in_specs=[anywhere] * 5 + [vmem] * 2,
        out_specs=vmem,
        scratch_shapes=[
            pltpu.VMEM((rows, width), bf),
            pltpu.VMEM((nx, 2, 2, wrows // 2, qcols), bf),
            pltpu.VMEM((nx, 2, wrows, kcols), bf),
            pltpu.VMEM((nx, 2, wrows, kcols), bf),
            pltpu.VMEM((nx, 2, 2, odepth // 2, ocols), bf),
            pltpu.VMEM((nz, rows, kcols), bf),
            pltpu.VMEM((nz, rows, kcols), bf),
            pltpu.VMEM((KV_HEADS, VROWS, keys), bf),
            pltpu.VMEM((KV_HEADS, 2 * HEAD_DIM, cols), bf),
            pltpu.VMEM((rows, qcols), f32),
            pltpu.VMEM((2, HALF, cols), f32),
            pltpu.VMEM((KV_HEADS, VROWS, cols), f32),
            pltpu.VMEM((KV_HEADS, 1, cols), f32),
            pltpu.VMEM((rows, qcols), bf),
            dma((3, 2, nx // 2, 2)),
            dma((3,)),
            dma((4,)),
            dma((4,)),
            dma((2, nz // 2, 2)),
            dma((2,)),
            dma((7,)),
        ],
        compiler_params=pltpu.CompilerParams(
            collective_id=0, has_side_effects=True, vmem_limit_bytes=50 * 1024 * 1024
        ),
    )(tokens, query_weight, key_weight, value_weight, out_weight,
      query_gain.reshape(1, -1), key_gain.reshape(1, -1))


def solution(mesh):
    nx, nz = mesh.shape["dp"] // 2, mesh.shape["sp"]
    in_specs = (
        P(("grp", "dp"), "sp", None),
        P("dp", None),
        P("dp", None),
        P("dp", None),
        P(None, "dp"),
        P(),
        P(),
    )
    out_specs = P(("grp", "dp"), "sp", None)

    def body(*args):
        return shards(nx, nz, *args)

    return jax.shard_map(body, mesh=mesh, in_specs=in_specs, out_specs=out_specs, check_vma=False)
```

time: 243 us -> 143 us (0.59)
  waiting for transfers between devices: 179 us -> 0 us
  Pallas kernels: 0 us -> 137 us
  matrix products: 30.5 us -> 0 us
  between operations: 13.3 us -> 0.02 us
  other arithmetic: 10.2 us -> 0 us
  local copies, waits for them, and re-layouts: 8.79 us -> 6.17 us
    all_gather x3 -> x0, waiting for transfers between devices: 178 us -> none  [the longest x1 88.1 us: sent_together(): lax.all_gather(both, axis, axis=dim, tiled=True)]
    pallas_call x0 -> x1, Pallas kernels: none -> 137 us  [shards(): pl.pallas_call(lambda *refs: kernel(nx, nz, *refs), out_shape=jax.ShapeDt...]
    dot_general x12 -> x0, matrix products: 30.5 us -> none  [the longest x4 11.6 us: attend_block(): jnp.einsum('kgqs,skd->qkgd', probs, values, preferred_element_type=jnp.fl...]
    unnamed x6 -> x15, local copies, waits for them, and re-layouts: 0.01 us -> 6.17 us
    reduce_sum x6 -> x0, other arithmetic: 5.33 us -> none  [the longest x4 4.88 us: attend_block(): jnp.sum(weights, axis=-1, keepdims=True)]
    slice x3 -> x0, local copies, waits for them, and re-layouts: 4.22 us -> none  [the longest x2 2.63 us: shards(): whole_kv[:, 0].reshape(length, KV_HEADS, HEAD_DIM).transpose(1, 0, 2)]
    dynamic_update_slice x4 -> x0, local copies, waits for them, and re-layouts: 2.68 us -> none  [shards(): per_head = lax.map(kv_head, (grouped_q, all_k, all_v))]
  transfers between devices with their start and end apart: 3 -> 0, of which waited for: 3 -> 0; matrix products, arithmetic and copies ran while one was open for 16% -> 0% of each run, Pallas kernels for 0% -> 0%
where the time goes in v1:
time: 143 us
  Pallas kernels  137 us (96%)
  local copies, waits for them, and re-layouts  6.17 us (4%)
    pallas_call x1, Pallas kernels, shards(): pl.pallas_call(lambda *refs: kernel(nx, nz, *refs), out_shape=jax.ShapeDt...  137 us
    unnamed x15, local copies, waits for them, and re-layouts  6.17 us

profile of v1, /device:TPU:65, one launch (start us, length us, event | category | flops | bytes accessed | tf_op | source)
XLA Modules:
  0.0 142.9 jit_solution(12232171698645676740)
XLA Ops:
  0.0 0.0 copy-start.5
  0.0 0.0 copy-start.6
  0.0 0.7 copy-done.5
  0.7 0.0 copy-done.6
  0.7 0.0 copy-start
  0.7 1.1 copy-done
  1.8 0.0 copy-start.1
  1.8 0.9 copy-done.1
  2.7 0.0 copy-start.2
  2.7 0.9 copy-done.2
  3.7 0.0 copy-start.3
  3.7 0.8 copy-done.3
  4.5 0.0 copy-start.4
  4.5 0.8 copy-done.4
  5.3 136.7 %shard_map.73 = bf16[1,160,2048]{2,1,0:T(8,128)(2,1)S(1)} custom-call(bf16[1,160,2048]{2,1,0:T(8,128)(2,1)S(1)} %copy-done, bf16[128,1024]{1,0:T(8,128)(2,1)S(1)} %copy-done.1, bf16[128,256]{1,0:T(8,128)(2,1)S(1)} %copy-done.3, bf16[128,256]{1,0:T(8,128)(2,1)S(1)} %copy-done.4, bf16[1024,128]{1,0:T(8,128)(2,1)S(1)} %copy-done.2, f32[1,64]{1,0:T(1,128)S(1)} %bitcast.2, ...), custom_call_target="tpu_custom_call" | custom-call | tf_op jit(solution)/shard_map/pallas_call | solution.py:366
  142.0 0.8 copy.9
Async XLA Ops:
  0.0 0.7 copy-start.5
  0.0 0.7 copy-start.6
  0.7 1.1 copy-start
  1.8 0.9 copy-start.1
  2.7 0.9 copy-start.2
  3.7 0.8 copy-start.3
  4.5 0.8 copy-start.4

commit v2 on v1

v2 whole, which is shorter than its diff:
```python
import math

import jax
import jax.numpy as jnp
from jax import lax
from jax.experimental import pallas as pl
from jax.experimental.pallas import tpu as pltpu
from jax.sharding import PartitionSpec as P

HEADS = 16
KV_HEADS = 4
HEAD_DIM = 64
GRID_W = 64
PER_KV = HEADS // KV_HEADS
HALF = HEAD_DIM // 2
QUARTER = HEAD_DIM // 4

theta_base = 10000.0
norm_eps = 1e-06
MESH = pl.DeviceIdType.MESH
LIMIT = 63 * 1024 * 1024
ONES = 16
VROWS = HEAD_DIM + ONES

PARTS = (
    None,
    (("all", 1 / 4), ("all", 1 / 4), ("own", 1 / 4)),
    (("all", 1 / 4), ("own", 3 / 16), ("own", 3 / 16)),
)

KV_AT, KV_STEP, KV_CUT = 2.8, 3.2, 0.7
Q_AT, Q_STEP, Q_CUT = 15.0, 4.2, 1.4
O_AT, O_STEP, O_CUT = 30.0, 3.6, 1.2
Y_LATE = 4.0
Z_AT, Z_STEP, Z_CUT = 19.0, 3.5, 0.85
X_MARGIN, Z_EARLY = 0.2, 0.2
KV_US, Q_US, UNIT_US = 1.5, 0.7, 0.4


def norm_rotate_t(raw, gain, cosine, sine):
    inv = lax.rsqrt(jnp.mean(raw * raw, axis=0, keepdims=True) + norm_eps)
    scaled = raw * inv * gain
    first, second = scaled[:HALF], scaled[HALF:]
    return jnp.concatenate(
        [first * cosine - second * sine, second * cosine + first * sine], axis=0
    )


def n_pieces(cls):
    return 4 if cls == 0 else len(PARTS[cls])


def far_way(cls, p):
    return int(p >= 2) if cls == 0 else int(p >= 1)


def make_schedule(nx, nz):
    h, hz = nx // 2, nz // 2
    xy, along_z = [], []
    timing = ((KV_AT, KV_STEP, KV_CUT), (Q_AT, Q_STEP, Q_CUT), (O_AT, O_STEP, O_CUT))
    for cls, (first, step, gap) in enumerate(timing):
        for s in range(1, h + 1):
            for d in range(2):
                count = 0
                for p in range(n_pieces(cls)):
                    if s == h and far_way(cls, p) != d:
                        continue
                    at = first + (s - 1) * step + gap * count
                    count += 1
                    xy.append((at, "w", cls, d, s, p))
                    if cls and PARTS[cls][p][0] == "own":
                        xy.append((at + Y_LATE, "y", cls, d, s, p))
    for s in range(1, hz + 1):
        for d in range(2):
            count = 0
            for p in range(4):
                if s == hz and far_way(0, p) != d:
                    continue
                along_z.append((Z_AT + (s - 1) * Z_STEP + Z_CUT * count, "z", d, s, p))
                count += 1
    return sorted(xy, key=lambda e: e[0]), sorted(along_z, key=lambda e: e[0])


def kernel(nx, nz, tok_in, wq_in, wk_in, wv_in, wo_in, qg_in, kg_in, out_ref,
           tok, wq, wk, wv, wo, kbuf, vbuf, vt, qbd, tab, acc, top, sbuf, pbuf, fade, att,
           ring_recv, ring_send, d2d_recv, d2d_send, z_recv, z_send, y_recv, y_send, loc):
    h_x, h_z = nx // 2, nz // 2
    rows = tok.shape[0]
    cols = PER_KV * rows
    dp = lax.axis_index("dp")
    z = lax.axis_index("sp")
    x, c = dp // 2, lax.rem(dp, 2)
    other = 1 - c
    to_x = ({"dp": lax.rem(dp + 2, 2 * nx)}, {"dp": lax.rem(dp + 2 * nx - 2, 2 * nx)})
    to_z = ({"sp": lax.rem(z + 1, nz)}, {"sp": lax.rem(z + nz - 1, nz)})
    to_core = {"dp": 2 * x + other}
    grp = lax.axis_index("grp")
    share = lax.rem(grp, 2)
    to_pair = {"grp": grp + 1 - 2 * share}

    wrows = wk.shape[2]
    loads = []

    def load(src, dst):
        cp = pltpu.make_async_copy(src, dst, loc.at[len(loads)])
        cp.start()
        loads.append(cp)

    load(wk_in, wk.at[x, c])
    load(wv_in, wv.at[x, c])
    load(tok_in.at[0], tok)
    load(wq_in, wq.at[x, c])
    load(wo_in, wo.at[x, c])

    barrier = pltpu.get_barrier_semaphore()
    for peer in (*to_x, *to_z, to_core, to_pair):
        pl.semaphore_signal(barrier, inc=1, device_id=peer, device_id_type=MESH)

    t = lax.broadcasted_iota(jnp.int32, (HALF, cols), 1)
    for _ in range(PER_KV - 1):
        t = jnp.where(t >= rows, t - rows, t)
    pos = z * rows + t
    j = lax.broadcasted_iota(jnp.int32, (HALF, cols), 0)
    on_row = j < QUARTER
    freq = jnp.exp(jnp.where(on_row, j, j - QUARTER).astype(jnp.float32) * (-math.log(theta_base) / QUARTER))
    angle = jnp.where(on_row, pos // GRID_W, lax.rem(pos, GRID_W)).astype(jnp.float32) * freq
    tab[0] = jnp.cos(angle)
    tab[1] = jnp.sin(angle)
    diag = lax.broadcasted_iota(jnp.int32, (HEAD_DIM, HEAD_DIM), 0) == lax.broadcasted_iota(
        jnp.int32, (HEAD_DIM, HEAD_DIM), 1
    )

    def column(ref):
        return jnp.sum(jnp.where(diag, ref[...], 0.0), axis=1, keepdims=True)

    vt[:, :, HEAD_DIM:, :] = jnp.ones((2, KV_HEADS, ONES, vt.shape[3]), jnp.bfloat16)
    qbd[...] = jnp.zeros(qbd.shape, jnp.bfloat16)
    acc[...] = jnp.zeros(acc.shape, jnp.float32)
    top[...] = jnp.full(top.shape, -1e30, jnp.float32)

    with jax.named_scope('barrier'):
        pl.semaphore_wait(barrier, 6)

    def cut(cls, p, theirs=False):
        total = (wq, wo)[cls - 1].shape[2]
        sizes = [int(total * f) for _, f in PARTS[cls]]
        kinds = [k for k, _ in PARTS[cls]]
        start, size = sum(sizes[:p]), sizes[p]
        if kinds[p] == "all":
            return start, size
        own = sum(n for n, k in zip(sizes, kinds) if k == "own")
        return pl.multiple_of(start + own * (1 - share if theirs else share), 16), size

    def piece(cls, xi, p, theirs=False):
        if cls == 0:
            return (wk, wv)[p % 2].at[xi, c, pl.ds((p // 2) * (wrows // 2), wrows // 2)]
        start, size = cut(cls, p, theirs)
        return (wq, wo)[cls - 1].at[xi, c, pl.ds(start, size)]

    def lane(cls, p):
        return cls + 1 if cls else p % 2

    def ring_copy(cls, d, s, p):
        owner = lax.rem(x + (nx - s + 1 if d == 0 else s - 1), nx)
        ref = piece(cls, owner, p)
        return pltpu.make_async_remote_copy(
            src_ref=ref, dst_ref=ref, send_sem=ring_send.at[cls],
            recv_sem=ring_recv.at[cls, d, s - 1, p],
            device_id=to_x[d], device_id_type=MESH,
        )

    def core_copy(lane_id, ref):
        pltpu.make_async_remote_copy(
            src_ref=ref, dst_ref=ref, send_sem=d2d_send.at[lane_id], recv_sem=d2d_recv.at[lane_id],
            device_id=to_core, device_id_type=MESH,
        ).start()

    def start_own(cls):
        for p in range(n_pieces(cls)):
            for d in range(2):
                ring_copy(cls, d, 1, p).start()
        if cls == 0:
            core_copy(0, wk.at[x, c])
            core_copy(1, wv.at[x, c])
        else:
            core_copy(cls + 1, (wq, wo)[cls - 1].at[x, c])

    def owner_of(d, s):
        return lax.rem(x + (nx - s if d == 0 else s), nx)

    def arrive_y(cls, d, s, p):
        ref = piece(cls, owner_of(d, s), p, theirs=True)
        pltpu.make_async_copy(ref, ref, y_recv.at[cls - 1, d, s - 1, p]).wait()
        core_copy(lane(cls, p), ref)

    def arrive_w(cls, d, s, p):
        ref = piece(cls, owner_of(d, s), p)
        pltpu.make_async_copy(ref, ref, ring_recv.at[cls, d, s - 1, p]).wait()
        if s + 1 < h_x or (s + 1 == h_x and far_way(cls, p) == d):
            ring_copy(cls, d, s + 1, p).start()
        if cls and PARTS[cls][p][0] == "own":
            pltpu.make_async_remote_copy(
                src_ref=ref, dst_ref=ref, send_sem=y_send.at[cls - 1],
                recv_sem=y_recv.at[cls - 1, d, s - 1, p],
                device_id=to_pair, device_id_type=MESH,
            ).start()
        core_copy(lane(cls, p), ref)

    def z_slot(d, s):
        return 0 if s == 0 else (2 * s - 1 if d == 0 or s == h_z else 2 * s)

    def z_piece(slot, p):
        return (vbuf, kbuf)[p // 2].at[slot, pl.ds((p % 2) * (rows // 2), rows // 2)]

    def z_send_piece(d, s, p):
        pltpu.make_async_remote_copy(
            src_ref=z_piece(z_slot(d, s - 1), p), dst_ref=z_piece(z_slot(d, s), p),
            send_sem=z_send.at[p // 2], recv_sem=z_recv.at[d, s - 1, p],
            device_id=to_z[d], device_id_type=MESH,
        ).start()

    def arrive_z(d, s, p):
        ref = z_piece(z_slot(d, s), p)
        pltpu.make_async_copy(ref, ref, z_recv.at[d, s - 1, p]).wait()
        if s + 1 < h_z or (s + 1 == h_z and far_way(0, p) == d):
            z_send_piece(d, s + 1, p)

    def core_wait(i):
        ref = (wk.at[:, other], wv.at[:, other], wq.at[:, other], wo.at[:, other])[i]
        pltpu.make_async_copy(ref, ref, d2d_recv.at[i]).wait()

    def project(weight):
        total = jnp.zeros((rows, weight.shape[-1]), jnp.float32)
        for i in range(nx):
            total += jnp.dot(
                tok[:, 2 * wrows * i:2 * wrows * (i + 1)],
                weight[i].reshape(2 * wrows, weight.shape[-1]),
                preferred_element_type=jnp.float32,
            )
        return total

    def make_kv():
        core_wait(1)
        vbuf[0] = project(wv).astype(jnp.bfloat16)
        core_wait(0)
        raw = project(wk)
        width = KV_HEADS * HEAD_DIM
        padded = jnp.concatenate([raw, jnp.zeros((width - rows, width), jnp.float32)], axis=0).T
        gain = column(kg_in)
        cosine, sine = tab[0, :, :width], tab[1, :, :width]
        turned = jnp.concatenate(
            [
                norm_rotate_t(padded[HEAD_DIM * i:HEAD_DIM * (i + 1)], gain, cosine, sine)
                for i in range(KV_HEADS)
            ],
            axis=0,
        ).T
        kbuf[0] = turned[:rows].astype(jnp.bfloat16)
        for p in range(4):
            for d in range(2):
                z_send_piece(d, 1, p)

    def make_q(g):
        at = slice(2 * 128 * g, 2 * 128 * (g + 1))
        total = jnp.zeros((rows, 256), jnp.float32)
        for i in range(nx):
            total += jnp.dot(
                tok[:, 2 * wrows * i:2 * wrows * (i + 1)],
                wq[i, :, :, at].reshape(2 * wrows, 256),
                preferred_element_type=jnp.float32,
            )
        both = jnp.concatenate([total[:, :128], total[:, 128:]], axis=0)
        stacked = jnp.concatenate([both, pltpu.roll(both, 64, 1)], axis=0)
        raw = stacked.T[:HEAD_DIM]
        at = (g % 2) * HEAD_DIM
        turned = norm_rotate_t(raw, column(qg_in), tab[0], tab[1])
        qbd[g, at:at + HEAD_DIM, :] = turned.astype(jnp.bfloat16)

    factor = HEAD_DIM ** (-0.5) * math.log2(math.e)
    edges = list(range(0, cols, 256)) + [cols]

    keys = 2 * rows

    def load_v(u):
        v = vbuf[2 * u:2 * u + 2].reshape(keys, KV_HEADS * HEAD_DIM).astype(jnp.float32)
        v = jnp.concatenate([v, jnp.zeros((vt.shape[3] - keys, v.shape[1]), jnp.float32)], axis=0)
        v = v.T.astype(jnp.bfloat16)
        for g in range(KV_HEADS):
            vt[u % 2, g, :HEAD_DIM, :] = v[HEAD_DIM * g:HEAD_DIM * (g + 1)]

    def attend(n):
        last = h_z * KV_HEADS
        for a, b in zip(edges[:-1], edges[1:]):
            if n >= 2:
                u, g = divmod(n - 2, KV_HEADS)
                o = jnp.dot(vt[u % 2, g, :, :keys], pbuf[n % 2, :, a:b], preferred_element_type=jnp.float32)
                acc[g, :, a:b] = acc[g, :, a:b] * fade[n % 2, :, a:b] + o
            if 1 <= n <= last:
                g = (n - 1) % KV_HEADS
                s = sbuf[(n - 1) % 2, :, a:b]
                pbuf[(n - 1) % 2, :, a:b] = jnp.exp2(s * factor - top[g, :, a:b]).astype(jnp.bfloat16)
            if n < last:
                u, g = divmod(n, KV_HEADS)
                at = (g // 2) * 128
                k = kbuf[2 * u:2 * u + 2, :, at:at + 128].reshape(keys, 128)
                s = jnp.dot(k, qbd[g, :, a:b], preferred_element_type=jnp.float32)
                old = top[g, :, a:b]
                new = jnp.maximum(old, jnp.max(s, axis=0, keepdims=True) * factor)
                sbuf[n % 2, :, a:b] = s
                fade[n % 2, :, a:b] = jnp.exp2(old - new)
                top[g, :, a:b] = new

    def finish():
        for g in range(KV_HEADS):
            o = acc[g, :HEAD_DIM] / acc[g, HEAD_DIM:HEAD_DIM + 1]
            o = jnp.concatenate([o, jnp.zeros((128 - HEAD_DIM, cols), jnp.float32)], axis=0).T
            y = (o[:2 * rows] + pltpu.roll(o[2 * rows:], 64, 1)).astype(jnp.bfloat16)
            att[:, 256 * g:256 * g + 128] = y[:rows]
            att[:, 256 * g + 128:256 * g + 256] = y[rows:]

    def project_out():
        core_wait(3)
        width = 2 * wo.shape[-1]

        for i in range(nx):
            w = jnp.concatenate([wo[i, 0], wo[i, 1]], axis=1)
            out_ref[0, :, i * width:(i + 1) * width] = jnp.dot(
                att[...], w, preferred_element_type=jnp.float32
            ).astype(jnp.bfloat16)

    with jax.named_scope('loads'):
        loads[0].wait()
        loads[1].wait()
    start_own(0)
    for cp in loads[2:]:
        cp.wait()

    xy, along_z = make_schedule(nx, nz)
    left = [sum(e[2] == cls for e in xy) for cls in range(3)]
    forwards = [sum(e[1] == "w" and e[2] == cls and e[4] < h_x for e in xy) for cls in range(3)]
    seen, clock = set(), 0.0
    q_work, steps, all_steps = [], 0, h_z * KV_HEADS + 2

    def unit_ready(u):
        return all(
            ("z", d, s, p) in seen
            for s in range(1, h_z + 1) for d in range(2) for p in range(4)
            if z_slot(d, s) // 2 == u and (s < h_z or far_way(0, p) == d)
        )

    def do_xy(e):
        _, kind, cls, d, s, p = e
        with jax.named_scope(f'{kind}{cls}{d}{s}{p}'):
            (arrive_w if kind == "w" else arrive_y)(cls, d, s, p)
        left[cls] -= 1
        if kind == "w" and s < h_x:
            forwards[cls] -= 1
            if forwards[cls] == 0 and cls < 2:
                start_own(cls + 1)
        if left[cls] == 0 and cls == 0:
            with jax.named_scope('make_kv'):
                make_kv()
            return KV_US
        if left[cls] == 0 and cls == 1:
            q_work.extend(range(KV_HEADS + 1))
        return 0.03

    def next_work():
        nonlocal steps
        if q_work:
            g = q_work.pop(0)
            with jax.named_scope(f'q{g}'):
                if g == 0:
                    core_wait(2)
                else:
                    make_q(g - 1)
            return Q_US if g else 0.05
        n, steps = steps, steps + 1
        u, g = divmod(n, KV_HEADS)
        with jax.named_scope(f'a{u}{g}'):
            if g == 0 and u < h_z:
                load_v(u)
            attend(n)
        return UNIT_US

    def has_work():
        if q_work:
            return True
        u = steps // KV_HEADS
        return left[1] == 0 and steps < all_steps and (u >= h_z or unit_ready(u))

    while xy or along_z or has_work():
        if along_z and left[0] == 0 and along_z[0][0] <= clock + Z_EARLY:
            e = along_z.pop(0)
        elif xy and xy[0][0] + X_MARGIN <= clock:
            e = xy.pop(0)
        elif has_work():
            clock += next_work()
            continue
        elif along_z and left[0] == 0 and (not xy or along_z[0][0] < xy[0][0] + X_MARGIN):
            e = along_z.pop(0)
        else:
            e = xy.pop(0)
        clock = max(clock, e[0])
        if e[1] == "z":
            with jax.named_scope(f'z{e[2]}{e[3]}{e[4]}'):
                arrive_z(*e[2:])
            seen.add(e[1:])
        else:
            clock += do_xy(e)
    with jax.named_scope('finish'):
        finish()
    with jax.named_scope('out'):
        project_out()

    def drain(ref, sem):
        pltpu.make_async_copy(ref, ref, sem).wait()

    drain(wk.at[0:nx - 1], ring_send.at[0])
    for i, w in enumerate((wq, wo)):
        sent = sum(cut(i + 1, p)[1] for p in range(n_pieces(i + 1)))
        part = sum(cut(i + 1, p)[1] for p, (k, _) in enumerate(PARTS[i + 1]) if k == "own")
        drain(w.at[0:nx - 1, 0, 0:sent], ring_send.at[i + 1])
        drain(w.at[0:nx - 1, 0, 0:part], y_send.at[i])
    for i, ref in enumerate((wk, wv, wq, wo)):
        drain(ref.at[:, c], d2d_send.at[i])
    drain(vbuf.at[0:nz - 1], z_send.at[0])
    drain(kbuf.at[0:nz - 1], z_send.at[1])


def shards(nx, nz, tokens, query_weight, key_weight, value_weight, out_weight, query_gain, key_gain):
    rows, width = tokens.shape[1], tokens.shape[2]
    wrows, qcols = query_weight.shape
    kcols = key_weight.shape[1]
    odepth, ocols = out_weight.shape
    cols = PER_KV * rows
    keys = -(-2 * rows // 128) * 128
    bf, f32 = jnp.bfloat16, jnp.float32
    dma = pltpu.SemaphoreType.DMA
    hbm = pl.BlockSpec(memory_space=pltpu.HBM)
    vmem = pl.BlockSpec(memory_space=pltpu.VMEM)
    return pl.pallas_call(
        lambda *refs: kernel(nx, nz, *refs),
        out_shape=jax.ShapeDtypeStruct(tokens.shape[:2] + (2 * nx * ocols,), bf),
        in_specs=[hbm] * 5 + [vmem] * 2,
        out_specs=vmem,
        scratch_shapes=[
            pltpu.VMEM((rows, width), bf),
            pltpu.VMEM((nx, 2, wrows, qcols), bf),
            pltpu.VMEM((nx, 2, wrows, kcols), bf),
            pltpu.VMEM((nx, 2, wrows, kcols), bf),
            pltpu.VMEM((nx, 2, odepth, ocols), bf),
            pltpu.VMEM((nz, rows, kcols), bf),
            pltpu.VMEM((nz, rows, kcols), bf),
            pltpu.VMEM((2, KV_HEADS, VROWS, keys), bf),
            pltpu.VMEM((KV_HEADS, 2 * HEAD_DIM, cols), bf),
            pltpu.VMEM((2, HALF, cols), f32),
            pltpu.VMEM((KV_HEADS, VROWS, cols), f32),
            pltpu.VMEM((KV_HEADS, 1, cols), f32),
            pltpu.VMEM((2, 2 * rows, cols), f32),
            pltpu.VMEM((2, 2 * rows, cols), bf),
            pltpu.VMEM((2, 1, cols), f32),
            pltpu.VMEM((rows, qcols), bf),
            dma((3, 2, nx // 2, 4)),
            dma((3,)),
            dma((4,)),
            dma((4,)),
            dma((2, nz // 2, 4)),
            dma((2,)),
            dma((2, 2, nx // 2, 3)),
            dma((2,)),
            dma((5,)),
        ],
        compiler_params=pltpu.CompilerParams(
            collective_id=0, has_side_effects=True, vmem_limit_bytes=LIMIT
        ),
    )(tokens, query_weight, key_weight, value_weight, out_weight,
      query_gain.reshape(1, -1), key_gain.reshape(1, -1))


def solution(mesh):
    nx, nz = mesh.shape["dp"] // 2, mesh.shape["sp"]
    in_specs = (
        P(("grp", "dp"), "sp", None),
        P("dp", None),
        P("dp", None),
        P("dp", None),
        P(None, "dp"),
        P(),
        P(),
    )
    out_specs = P(("grp", "dp"), "sp", None)

    def body(*args):
        return shards(nx, nz, *args)

    return jax.shard_map(body, mesh=mesh, in_specs=in_specs, out_specs=out_specs, check_vma=False)
```

time: 143 us -> 109 us (0.76)
  Pallas kernels: 137 us -> 107 us
  local copies, waits for them, and re-layouts: 6.17 us -> 1.98 us
    pallas_call x1, Pallas kernels: 137 us -> 107 us  [shards(): pl.pallas_call(lambda *refs: kernel(nx, nz, *refs), out_shape=jax.ShapeDt...]
    unnamed x15 -> x1, local copies, waits for them, and re-layouts: 6.17 us -> 1.98 us
where the time goes in v2:
time: 109 us
  Pallas kernels  107 us (98%)
  local copies, waits for them, and re-layouts  1.98 us (2%)
    pallas_call x1, Pallas kernels, shards(): pl.pallas_call(lambda *refs: kernel(nx, nz, *refs), out_shape=jax.ShapeDt...  107 us

profile of v2, /device:TPU:65, one launch (start us, length us, event | category | flops | bytes accessed | tf_op | source)
XLA Modules:
  0.0 109.0 jit_solution(12100976004958113934)
XLA Ops:
  0.0 107.0 %shard_map.73 = bf16[1,160,2048]{2,1,0:T(8,128)(2,1)} custom-call(bf16[1,160,2048]{2,1,0:T(8,128)(2,1)} %refs_0_.1, bf16[128,1024]{1,0:T(8,128)(2,1)} %refs_1_.1, bf16[128,256]{1,0:T(8,128)(2,1)} %refs_2_.1, bf16[128,256]{1,0:T(8,128)(2,1)} %refs_3_.1, bf16[1024,128]{1,0:T(8,128)(2,1)} %refs_4_.1, f32[1,64]{1,0:T(1,128)} %bitcast.2, f32[1,64]{1,0:T(1,128)} %bitcast.3), custom_call_target="tpu_custom_call" | custom-call | tf_op jit(solution)/shard_map/pallas_call | solution.py:442
  107.0 2.0 %copy.9 = bf16[1,160,2048]{2,1,0:T(8,128)(2,1)} copy(bf16[1,160,2048]{2,1,0:T(8,128)(2,1)} %shard_map.73) | data formatting | bytes 1310720
